TPU v7x, 32 devices: a whole 2x2x4 slice. The times are simulated.
32 devices in a mesh: sp: 2 (over x), dp: 16 (over z, y, core).
Axes of the slice: x: 2, y: 2, z: 4, core: 2. Of those that a mesh axis runs over, the one named last changes fastest.
Arguments:
- hidden_in: bfloat16 [1024, 2048], P('sp'), may hold values from -6 to 6
- content_weight: bfloat16 [2048, 2048], P('sp', 'dp'), may hold values from -0.125 to 0.125
- gating_weight: bfloat16 [2048, 2048], P('sp', 'dp'), may hold values from -2 to 2
- norm_gain: float32 [2048], P('dp'), may hold values from 0.1 to 1.9
- mixing_weight: bfloat16 [16, 128, 128], P('dp'), may hold values from -0.5 to 0.5
- mixing_bias: float32 [16, 128], P('dp'), may hold values from 0.1 to 1.9
- out_grad: bfloat16 [1024, 2048], P('sp', 'dp'), may hold values from -13 to 13
Outputs:
- input_grad: bfloat16 [1024, 2048], P('sp', 'dp')
- content_grad: float32 [2048, 2048], P('sp', 'dp')
- gating_grad: float32 [2048, 2048], P('sp', 'dp')
- mixing_grad: float32 [16, 128, 128], P('dp')
All inputs are finite; a program needn't handle non-finite values.
Results may differ from a plain program's by a relative error of at most 0.019.
Values may be sent and summed in bfloat16 or wider, within the bound.
A program may use at most 64 MiB of HBM per device.

v0:
```python
import math

import jax
import jax.numpy as jnp
from jax import lax
from jax.sharding import PartitionSpec as P

GROUP_DIM = 128
BLOCK = 128


norm_eps = 1e-05


def gelu_slope(values):
    cumulative = 0.5 * (1.0 + lax.erf(values * (1.0 / math.sqrt(2.0))))
    density = jnp.exp(-0.5 * values * values) * (1.0 / math.sqrt(2.0 * math.pi))
    return cumulative + values * density


def causal_table(weights):
    row_ids = lax.broadcasted_iota(jnp.int32, (BLOCK, BLOCK), 0)
    col_ids = lax.broadcasted_iota(jnp.int32, (BLOCK, BLOCK), 1)
    keeper = (col_ids <= row_ids)[None]
    return (jnp.where(keeper, weights, jnp.zeros_like(weights)), keeper)


def hidden_term(hidden_in, grads):
    return lax.dot_general(
        hidden_in, grads, (((0,), (0,)), ((), ())), preferred_element_type=jnp.float32
    )


def local(
    hidden_in, content_weight, gating_weight, norm_gain, mixing_weight, mixing_bias, out_grad
):
    tok_rows = hidden_in.shape[0]
    local_width = content_weight.shape[1]
    groups_here = local_width // GROUP_DIM
    blocks = tok_rows // BLOCK
    full_width = local_width * lax.axis_size("dp")
    grad_scale = 1.0 / math.sqrt(tok_rows * lax.axis_size("sp"))
    whole_content, whole_gating = (
        lax.all_gather(content_weight, "sp", axis=0, tiled=True),
        lax.all_gather(gating_weight, "sp", axis=0, tiled=True),
    )
    joined_weight = jnp.concatenate([whole_content, whole_gating], axis=1)
    pre_both = jnp.dot(hidden_in, joined_weight, preferred_element_type=jnp.float32).astype(
        jnp.bfloat16
    )
    pre_content = pre_both[:, :local_width].astype(jnp.float32)
    pre_gating = pre_both[:, local_width:].astype(jnp.float32)
    content = jax.nn.gelu(pre_content, approximate=False)
    gating = jax.nn.gelu(pre_gating, approximate=False)
    spatial, keeper = causal_table(mixing_weight)
    grad_wide = out_grad.astype(jnp.float32)
    mixed_grad = (grad_wide * content).astype(jnp.bfloat16)
    mixed_blocks = mixed_grad.reshape(blocks, BLOCK, groups_here, GROUP_DIM)
    normed_grad = jnp.einsum(
        "gts,btgc->bsgc", spatial, mixed_blocks, preferred_element_type=jnp.float32
    )
    centred_grad = normed_grad.reshape(tok_rows, local_width) * norm_gain[None, :]
    row_sum, row_square, grad_sum, grad_raw = lax.psum(
        (
            jnp.sum(gating, axis=1),
            jnp.sum(gating * gating, axis=1),
            jnp.sum(centred_grad, axis=1),
            jnp.sum(centred_grad * gating, axis=1),
        ),
        "dp",
    )
    row_mean = (row_sum / full_width)[:, None]
    row_var = (row_square / full_width)[:, None] - row_mean * row_mean
    inv_std = lax.rsqrt(row_var + norm_eps)
    centred = (gating - row_mean) * inv_std
    first_moment = (grad_sum / full_width)[:, None]
    second_moment = inv_std * ((grad_raw / full_width)[:, None] - row_mean * first_moment)
    normed = (centred * norm_gain[None, :]).astype(jnp.bfloat16)
    normed_blocks = normed.reshape(blocks, BLOCK, groups_here, GROUP_DIM)
    mixed = jnp.einsum("gts,bsgc->btgc", spatial, normed_blocks, preferred_element_type=jnp.float32)
    mixed = (mixed + jnp.transpose(mixing_bias)[None, :, :, None]).reshape(tok_rows, local_width)
    content_pre_grad = (grad_wide * mixed * gelu_slope(pre_content)).astype(jnp.bfloat16)
    local_mixing = jnp.einsum(
        "btgc,bsgc->gts", mixed_blocks, normed_blocks, preferred_element_type=jnp.float32
    )
    local_mixing = jnp.where(keeper, local_mixing, 0.0)
    mixing_grad = lax.psum(local_mixing.astype(jnp.bfloat16), "sp").astype(jnp.float32) * grad_scale
    gating_back = inv_std * (centred_grad - first_moment - centred * second_moment)
    gating_pre_grad = (gating_back * gelu_slope(pre_gating)).astype(jnp.bfloat16)
    joined_grad = jnp.concatenate([content_pre_grad, gating_pre_grad], axis=1)
    partial_input = lax.dot_general(
        joined_grad, joined_weight, (((1,), (1,)), ((), ())), preferred_element_type=jnp.float32
    )
    input_grad = lax.psum_scatter(
        partial_input.astype(jnp.bfloat16), "dp", scatter_dimension=1, tiled=True
    )
    both_grads = (
        lax.psum_scatter(
            hidden_term(hidden_in, joined_grad).astype(jnp.bfloat16),
            "sp",
            scatter_dimension=0,
            tiled=True,
        ).astype(jnp.float32)
        * grad_scale
    )
    content_grad = both_grads[:, :local_width]
    gating_grad = both_grads[:, local_width:]
    return (input_grad, content_grad, gating_grad, mixing_grad)


def solution(mesh):
    in_specs = (
        P("sp", None),
        P("sp", "dp"),
        P("sp", "dp"),
        P("dp"),
        P("dp", None, None),
        P("dp", None),
        P("sp", "dp"),
    )
    out_specs = (P("sp", "dp"), P("sp", "dp"), P("sp", "dp"), P("dp", None, None))
    return jax.shard_map(local, mesh=mesh, in_specs=in_specs, out_specs=out_specs, check_vma=False)
```

profile of v0, /device:TPU:0, one launch (start us, length us, event | category | flops | bytes accessed | tf_op | source)
XLA Modules:
  0.0 171.6 jit_solution(2205242992062746449)
XLA Ops:
  7.2 10.3 %all_gather.6 = bf16[2048,128]{1,0:T(8,128)(2,1)S(1)} all-gather(bf16[1024,128]{1,0:T(8,128)(2,1)} %param.8), channel_id=1, replica_groups=mesh['sp'=2,'dp'=16] {'sp'}, dimensions={0}, use_global_device_ids=true | all-gather | bytes 786432 | tf_op jit(solution)/shard_map/all_gather | solution.py:44
  17.6 0.1 constant_dynamic-update-slice_fusion.1
  17.7 9.8 %all_gather.7 = bf16[2048,128]{1,0:T(8,128)(2,1)} all-gather(bf16[1024,128]{1,0:T(8,128)(2,1)} %param.9), channel_id=1, replica_groups=mesh['sp'=2,'dp'=16] {'sp'}, dimensions={0}, use_global_device_ids=true | all-gather | bytes 786432 | tf_op jit(solution)/shard_map/all_gather | solution.py:45
  27.4 0.1 copy.21
  27.5 1.2 constant_dynamic-update-slice_fusion
  28.7 0.8 fusion.1
  29.5 0.7 copy-done.4
  30.2 0.6 fusion.8
  30.8 0.1 copy.38
  30.9 1.7 %fusion.82 = (f32[4,128]{1,0:T(4,128)S(1)}, f32[4,128,128]{1,2,0:T(8,128)}) fusion(f32[128]{0:T(128)S(1)} %copy-done.6, bf16[4,128,128]{2,1,0:T(8,128)(2,1)S(1)} %bitcast.53, bf16[1,128,128]{2,1,0:T(8,128)(2,1)} %param.11), kind=kOutput, calls=%fused_computation.106 | convolution fusion | flops 16940544 | bytes 428544 | tf_op jit(solution)/shard_map/gts,btgc->bsgc/dot_general | solution.py:59
  32.7 1.1 copy.34
  33.8 2.2 %fusion.95 = (f32[512]{0:T(512)S(1)}, f32[512]{0:T(512)S(1)}, f32[512]{0:T(512)S(1)}, f32[512,128]{0,1:T(8,128)}) fusion(f32[512,128]{0,1:T(8,128)S(1)} %copy.34, f32[128]{0:T(128)} %param.10, bf16[512,256]{0,1:T(8,128)(2,1)} %copy-done.4), kind=kLoop, calls=%fused_computation.130 | loop fusion | flops 4651520 | bytes 662016 | tf_op jit(solution)/shard_map/reduce_sum | solution.py:65
  36.0 33.1 %all-reduce = (f32[512]{0:T(512)}, f32[512]{0:T(512)}, f32[512]{0:T(512)}, f32[512]{0:T(512)}) all-reduce(f32[512]{0:T(512)S(1)} %get-tuple-element.13, f32[512]{0:T(512)S(1)} %get-tuple-element.14, f32[512]{0:T(512)S(1)} %bitcast.60, f32[512]{0:T(512)S(1)} %get-tuple-element.12), channel_id=1, replica_groups=mesh['sp'=2,'dp'=16] {'dp'}, use_global_device_ids=true, to_apply=%region_7.8 | all-reduce | flops 2048 | bytes 16384 | tf_op jit(solution)/shard_map/psum | solution.py:63
  69.1 0.7 add_rsqrt_fusion
  69.8 1.9 %multiply_convert_fusion = (bf16[512,128]{0,1:T(8,128)(2,1)}, bf16[512,128]{0,1:T(8,128)(2,1)}) fusion(f32[512,128]{0,1:T(8,128)} %get-tuple-element.19, f32[128]{0:T(128)} %param.10, f32[512]{0:T(512)S(1)} %get-tuple-element.24, f32[512]{0:T(512)S(1)} %get-tuple-element.27, bf16[512,256]{0,1:T(8,128)(2,1)} %copy-done.4, f32[512]{0:T(512)S(1)} %get-tuple-element.25, ...), kind=kLoop, calls=%fused_computation.108 | loop fusion | flops 1310720 | bytes 926208 | tf_op jit(solution)/shard_map/convert_element_type | solution.py:78
  71.7 1.0 copy.37
  72.8 1.6 fusion.2
  74.4 1.8 %copy.32 = f32[512,128]{0,1:T(8,128)} copy(f32[512,128]{1,0:T(8,128)} %bitcast.58) | data formatting | bytes 524288 | tf_op jit(solution)/shard_map/reshape | solution.py:81
  76.2 1.1 fusion.7
  77.3 2.7 %fusion = bf16[2048,256]{0,1:T(8,128)(2,1)} fusion(bf16[512,2048]{1,0:T(8,128)(2,1)S(1)} %copy-done, bf16[512,128]{0,1:T(8,128)(2,1)} %get-tuple-element.23, bf16[512,128]{0,1:T(8,128)(2,1)S(1)} %fusion.7), kind=kOutput, calls=%fused_computation.2 | convolution fusion | flops 537919488 | bytes 3407872 | tf_op jit(solution)/shard_map/dot_general | solution.py:29
  80.1 2.1 %convolution_convert_fusion = bf16[512,2048]{1,0:T(8,128)(2,1)} fusion(bf16[2048,256]{1,0:T(8,128)(2,1)S(1)} %constant_dynamic-update-slice_fusion, bf16[512,128]{0,1:T(8,128)(2,1)S(1)} %copy-done.3, bf16[512,128]{0,1:T(8,128)(2,1)S(1)} %fusion.7), kind=kOutput, calls=%fused_computation | convolution fusion | flops 538443776 | bytes 3407872 | tf_op jit(solution)/shard_map/dot_general | solution.py:91
  82.1 4.0 %copy.35 = bf16[512,2048]{0,1:T(8,128)(2,1)} copy(bf16[512,2048]{1,0:T(8,128)(2,1)} %convolution_convert_fusion) | data formatting | bytes 4194304
  86.1 0.9 copy-done.2
  87.0 0.2 fusion.5
  87.2 8.3 %psum.39 = bf16[1,128,128]{2,1,0:T(8,128)(2,1)S(1)} all-reduce(bf16[1,128,128]{2,1,0:T(8,128)(2,1)S(1)} %fusion.5), channel_id=1, replica_groups=mesh['sp'=2,'dp'=16] {'sp'}, use_global_device_ids=true, to_apply=%region_10.11 | all-reduce | flops 16384 | bytes 65536 | tf_op jit(solution)/shard_map/psum | solution.py:87
  95.5 0.6 convert_multiply_fusion.13
  96.1 1.4 reduce-scatter.5.cloned.1.call-done
  97.5 1.1 convert_multiply_fusion
  98.8 1.0 copy.29
  99.8 1.0 copy.30
  100.8 62.4 %reduce-scatter.7.cloned.1.call-done = bf16[128,512]{1,0:T(8,128)(2,1)} async-done(((bf16[2048,512]{1,0:T(8,128)(2,1)}), bf16[128,512]{1,0:T(8,128)(2,1)}) %reduce-scatter.7.cloned.1.call-update) | async-done | bytes 131088
  163.1 1.7 copy.36
  (17 shorter events, 0.2 us)
Async XLA Ops:
  7.2 21.6 %copy-start = (bf16[512,2048]{1,0:T(8,128)(2,1)S(1)}, bf16[512,2048]{1,0:T(8,128)(2,1)}, u32[]{:S(2)}) copy-start(bf16[512,2048]{1,0:T(8,128)(2,1)} %param.7) | copy-start | bytes 6291460
  7.2 20.2 %copy-start.5 = (bf16[512,128]{1,0:T(8,128)(2,1)S(1)}, bf16[512,128]{1,0:T(8,128)(2,1)}, u32[]{:S(2)}) copy-start(bf16[512,128]{1,0:T(8,128)(2,1)} %param.13) | copy-start | bytes 393220
  7.2 90.3 %reduce-scatter.5.cloned.1.call-start = ((), (), s32[]{:S(2)}) async-start(), calls=%async_computation.2 | async-start | bytes 1572864 | tf_op jit(solution)/shard_map/reduce_scatter | solution.py:98
  28.7 2.2 %copy-start.6 = (f32[128]{0:T(128)S(1)}, f32[128]{0:T(128)}, u32[]{:S(2)}) copy-start(f32[128]{0:T(128)} %param.10) | copy-start | bytes 1540
  29.5 0.7 copy-start.4
  30.9 1.8 %copy-start.1 = (bf16[512,128]{1,0:T(8,128)(2,1)}, bf16[512,128]{1,0:T(8,128)(2,1)S(1)}, u32[]{:S(2)}) copy-start(bf16[512,128]{1,0:T(8,128)(2,1)S(1)} %copy.38) | copy-start | bytes 393220
  77.3 2.7 %copy-start.3 = (bf16[512,128]{0,1:T(8,128)(2,1)S(1)}, bf16[512,128]{0,1:T(8,128)(2,1)}, u32[]{:S(2)}) copy-start(bf16[512,128]{0,1:T(8,128)(2,1)} %get-tuple-element.23) | copy-start | bytes 393220
  80.0 83.1 %reduce-scatter.7.cloned.1.call-start = ((), (), s32[]{:S(2)}) async-start(), calls=%async_computation.3 | async-start | bytes 2228224
  86.1 0.9 copy-start.2
Sparse Core Ops, SparseCore 0:
  80.1 17.3 reduce-scatter.4
  101.3 61.8 reduce-scatter.6
where the time goes:
time: 172 us
  waiting for transfers between devices  63.8 us (37%)
  blocking collectives  61.5 us (36%)
  local copies, waits for them, and re-layouts  14.7 us (9%)
  between operations  14.2 us (8%)
  matrix products  9.04 us (5%)
  other arithmetic  8.35 us (5%)
    unnamed x3, waiting for transfers between devices  62.4 us
    psum x1, blocking collectives, local(): lax.psum((jnp.sum(gating, axis=1), jnp.sum(gating * gating, axis=1), jnp....  33.1 us
    all_gather x1, blocking collectives, local(): lax.all_gather(content_weight, 'sp', axis=0, tiled=True)  10.3 us
    all_gather x1, blocking collectives, local(): lax.all_gather(gating_weight, 'sp', axis=0, tiled=True)  9.76 us
    unnamed x20, local copies, waits for them, and re-layouts  9.46 us
    psum x1, blocking collectives, local(): lax.psum(local_mixing.astype(jnp.bfloat16), 'sp').astype(jnp.float32)  8.27 us
  transfers between devices with their start and end apart: 2, of which 2 were waited for; matrix products, arithmetic and copies ran while one was open for 6% of the time, Pallas kernels for 0%

commit v1 on v0

--- a/solution.py
+++ b/solution.py
@@ -1,8 +1,11 @@
+import functools
 import math
 
 import jax
 import jax.numpy as jnp
 from jax import lax
+from jax.experimental import pallas as pl
+from jax.experimental.pallas import tpu as pltpu
 from jax.sharding import PartitionSpec as P
 
 GROUP_DIM = 128
@@ -108,6 +111,343 @@
     return (input_grad, content_grad, gating_grad, mixing_grad)
 
 
+def phi_and_slope(values):
+    cumulative = 0.5 * (1.0 + lax.erf(values * (1.0 / math.sqrt(2.0))))
+    density = jnp.exp(-0.5 * values * values) * (1.0 / math.sqrt(2.0 * math.pi))
+    return cumulative, cumulative + values * density
+
+
+def dot(a, b, ca, cb):
+    return lax.dot_general(
+        a, b, (((ca,), (cb,)), ((), ())), preferred_element_type=jnp.float32
+    )
+
+
+def fused_kernel(
+    n_dp, full_width, grad_scale,
+    h_in, wc_in, wg_in, gain_ref, mix_ref, bias_ref, og_in,
+    x_out, c_out, g_out, m_out,
+    hid, hid_t, wts, og, cg, cg_t, cs, gat, slope_g, mg, joined,
+    stat_a, stat_quad, stat_b, stat_z,
+    part, r_core, q_send, r_y, z_send, r_z, acc,
+    gs, gr, go, ms, mr,
+    load_sem, w_send, w_recv, sq_send, sq_recv, sz_send, sz_recv,
+    core_send, core_recv, y_send, y_recv, zz_send, zz_recv,
+    gx_send, gx_recv, mx_send, mx_recv,
+):
+    toks = hid.shape[0]
+    chunks = toks // BLOCK
+    shard = wc_in.shape[0]
+    nz = n_dp // 4
+    half = toks // 2
+    tiles = gs.shape[0]
+    tile = gs.shape[1]
+    bf16 = jnp.bfloat16
+    f32 = jnp.float32
+
+    i = lax.axis_index("sp")
+    j = lax.axis_index("dp")
+    x_peer = 1 - i
+    c = lax.rem(j, 2)
+    y = lax.rem(j // 2, 2)
+    z = j // 4
+    j_core = j + 1 - 2 * c
+    j_y = j + 2 - 4 * y
+    j_diag = j_core + 2 - 4 * y
+
+    def z_dev(q):
+        return lax.rem(z + q, nz) * 4 + y * 2 + c
+
+    def dev(a, b):
+        return {"sp": a, "dp": b}
+
+    def remote(src, dst, ssem, rsem, target):
+        return pltpu.make_async_remote_copy(
+            src_ref=src, dst_ref=dst, send_sem=ssem, recv_sem=rsem,
+            device_id=target, device_id_type=pl.DeviceIdType.MESH,
+        )
+
+    mine = pl.multiple_of(i * shard, shard)
+    theirs = pl.multiple_of(x_peer * shard, shard)
+    loads = [
+        pltpu.make_async_copy(wc_in, wts.at[pl.ds(mine, shard), pl.ds(0, BLOCK)], load_sem.at[0]),
+        pltpu.make_async_copy(h_in, hid, load_sem.at[1]),
+        pltpu.make_async_copy(wg_in, wts.at[pl.ds(mine, shard), pl.ds(BLOCK, BLOCK)], load_sem.at[2]),
+        pltpu.make_async_copy(og_in, og, load_sem.at[3]),
+    ]
+    for load in loads:
+        load.start()
+
+    barrier = pltpu.get_barrier_semaphore()
+    peers = [dev(x_peer, j), dev(i, j_core), dev(i, j_y), dev(i, j_diag)]
+    peers += [dev(i, z_dev(q)) for q in range(1, nz)]
+    for peer in peers:
+        pl.semaphore_signal(barrier, inc=1, device_id=peer, device_id_type=pl.DeviceIdType.MESH)
+    pl.semaphore_wait(barrier, len(peers))
+
+    pieces = w_send.shape[0] // 2
+    piece = shard // pieces
+    w_copies = []
+    for which, src in ((0, wc_in), (1, wg_in)):
+        for p in range(pieces):
+            copy = remote(
+                src.at[pl.ds(p * piece, piece), :],
+                wts.at[pl.ds(pl.multiple_of(mine + p * piece, piece), piece), pl.ds(which * BLOCK, BLOCK)],
+                w_send.at[which * pieces + p], w_recv.at[which * pieces + p],
+                dev(x_peer, j),
+            )
+            copy.start()
+            w_copies.append(copy)
+
+    keep = lax.broadcasted_iota(jnp.int32, (BLOCK, BLOCK), 1) <= lax.broadcasted_iota(
+        jnp.int32, (BLOCK, BLOCK), 0
+    )
+    spatial = jnp.where(keep, mix_ref[0].astype(f32), 0.0).astype(bf16)
+    gain = gain_ref[...]
+    bias = jnp.broadcast_to(bias_ref[...], (BLOCK, BLOCK)).T
+
+    for load in loads:
+        load.wait()
+    own = dot(hid[:, pl.ds(mine, shard)], wts[pl.ds(mine, shard), :], 1, 0)
+    joined_pre = own
+    acc_c = go.at[pl.ds(0, toks), pl.ds(0, BLOCK)]
+    acc_g = go.at[pl.ds(0, toks), pl.ds(BLOCK, BLOCK)]
+    go[pl.ds(0, toks), :] = joined_pre
+    for b in range(hid.shape[1] // BLOCK):
+        hid_t[pl.ds(b * BLOCK, BLOCK), :] = hid[:, pl.ds(b * BLOCK, BLOCK)].T
+
+    def finish(which, target):
+        for p in range(pieces):
+            w_copies[which * pieces + p].wait_recv()
+            at = pl.multiple_of(theirs + p * piece, piece)
+            target[...] += dot(
+                hid[:, pl.ds(at, piece)], wts[pl.ds(at, piece), pl.ds(which * BLOCK, BLOCK)], 1, 0
+            )
+
+    finish(0, acc_c)
+    for k in range(chunks):
+        rows = pl.ds(k * BLOCK, BLOCK)
+        pre = go[rows, 0:BLOCK].astype(bf16).astype(f32)
+        wide = og[rows, :].astype(f32)
+        cumulative, slope = phi_and_slope(pre)
+        cs[rows, :] = wide * slope
+        mixed_grad = (wide * (pre * cumulative)).astype(bf16)
+        mg[rows, :] = mixed_grad
+        centred_grad = dot(spatial, mixed_grad, 0, 0) * gain
+        cg[rows, :] = centred_grad
+        cg_t[rows, :] = centred_grad.T
+
+    finish(1, acc_g)
+    for k in range(chunks):
+        rows = pl.ds(k * BLOCK, BLOCK)
+        pre = go[rows, BLOCK:2 * BLOCK].astype(bf16).astype(f32)
+        cumulative, slope = phi_and_slope(pre)
+        gating = pre * cumulative
+        gat[rows, :] = gating
+        slope_g[rows, :] = slope
+        turned = gating.T
+        grad_turned = cg_t[rows, :]
+        base = 4 * (k * BLOCK // half)
+        cols = pl.ds(k * BLOCK % half, BLOCK)
+        for row, table in enumerate((turned, turned * turned, grad_turned, grad_turned * turned)):
+            stat_a[base + row:base + row + 1, cols] = jnp.sum(table, axis=0, keepdims=True)
+
+    stat_copies = []
+    for s, target in enumerate((j_core, j_y, j_diag)):
+        copy = remote(stat_a, stat_quad.at[s], sq_send.at[s], sq_recv.at[s], dev(i, target))
+        copy.start()
+        stat_copies.append(copy)
+    for copy in stat_copies:
+        copy.wait()
+    stat_b[...] = (stat_a[...] + stat_quad[0]) + (stat_quad[1] + stat_quad[2])
+    stat_copies = []
+    for q in range(1, nz):
+        copy = remote(
+            stat_b, stat_z.at[q - 1], sz_send.at[q - 1], sz_recv.at[q - 1], dev(i, z_dev(q))
+        )
+        copy.start()
+        stat_copies.append(copy)
+    for copy in stat_copies:
+        copy.wait()
+    total = stat_b[...]
+    for q in range(1, nz):
+        total = total + stat_z[q - 1]
+    total = total * (1.0 / full_width)
+
+    mixing = jnp.zeros((BLOCK, BLOCK), f32)
+    for k in range(chunks):
+        rows = pl.ds(k * BLOCK, BLOCK)
+        base = 4 * (k * BLOCK // half)
+        col = k * BLOCK % half
+        part_of = total[base:base + 4, col:col + BLOCK]
+        mean = part_of[0:1]
+        inv = lax.rsqrt(part_of[1:2] - mean * mean + norm_eps)
+        first = part_of[2:3]
+        second = inv * (part_of[3:4] - mean * first)
+
+        def spread(row):
+            return jnp.broadcast_to(row, (BLOCK, BLOCK)).T
+
+        inv_w = spread(inv)
+        centred = (gat[rows, :] - spread(mean)) * inv_w
+        normed = (centred * gain).astype(bf16)
+        mixed = dot(spatial, normed, 1, 0) + bias
+        joined[rows, 0:BLOCK] = (cs[rows, :] * mixed).astype(bf16)
+        back = inv_w * (cg[rows, :] - spread(first) - centred * spread(second))
+        joined[rows, BLOCK:2 * BLOCK] = (back * slope_g[rows, :]).astype(bf16)
+        mixing = mixing + dot(mg[rows, :], normed, 1, 1)
+    mixing = jnp.where(keep, mixing, 0.0)
+
+    waits = []
+
+    def input_part(k):
+        grads = joined[pl.ds(k * BLOCK, BLOCK), :]
+        for zz in range(nz):
+            res = dot(grads, wts[pl.ds(zz * 4 * BLOCK, 4 * BLOCK), :], 1, 1).astype(bf16)
+            for yy in range(2):
+                for cc in range(2):
+                    at = (yy * 2 + cc) * BLOCK
+                    part[k, cc, yy, zz] = res[:, at:at + BLOCK]
+        copy = remote(part.at[k, 1 - c], r_core.at[k], core_send.at[k], core_recv.at[k], dev(i, j_core))
+        copy.start()
+        waits.append(copy)
+        return copy
+
+    def weight_part(t):
+        at = pl.multiple_of(theirs + t * tile, tile)
+        gs[t] = dot(hid_t[pl.ds(at, tile), :], joined[...], 1, 0).astype(bf16)
+        copy = remote(gs.at[t], gr.at[t], gx_send.at[t], gx_recv.at[t], dev(x_peer, j))
+        copy.start()
+        waits.append(copy)
+        return copy
+
+    core_copies, y_copies, z_copies, g_copies = {}, {}, {}, {}
+
+    def second_stage(k):
+        core_copies[k].wait_recv()
+        q_send[k] = (
+            part[k, c, 1 - y].astype(f32) + r_core[k, 1 - y].astype(f32)
+        ).astype(bf16)
+        copy = remote(q_send.at[k], r_y.at[k], y_send.at[k], y_recv.at[k], dev(i, j_y))
+        copy.start()
+        waits.append(copy)
+        y_copies[k] = copy
+
+    def third_stage(k):
+        y_copies[k].wait_recv()
+        z_copies[k] = []
+        for q in range(1, nz + 1):
+            zt = lax.rem(z + q, nz)
+            res = (
+                part[k, c, y, zt].astype(f32) + r_core[k, y, zt].astype(f32)
+            ) + r_y[k, zt].astype(f32)
+            if q == nz:
+                acc[k] = res
+                continue
+            z_send[k, q - 1] = res.astype(bf16)
+            copy = remote(
+                z_send.at[k, q - 1], r_z.at[k, q - 1], zz_send.at[k, q - 1], zz_recv.at[k, q - 1],
+                dev(i, z_dev(q)),
+            )
+            copy.start()
+            waits.append(copy)
+            z_copies[k].append(copy)
+
+    def last_stage(k):
+        res = acc[k]
+        for q in range(1, nz):
+            z_copies[k][q - 1].wait_recv()
+            res = res + r_z[k, q - 1].astype(f32)
+        x_out[pl.ds(k * BLOCK, BLOCK), :] = res.astype(bf16)
+
+    for step in range(max(chunks + 2, tiles)):
+        if step < chunks:
+            core_copies[step] = input_part(step)
+        if step < tiles:
+            g_copies[step] = weight_part(step)
+        if 0 <= step - 1 < chunks:
+            second_stage(step - 1)
+        if 0 <= step - 2 < chunks:
+            third_stage(step - 2)
+    ms[...] = mixing.astype(bf16)
+    m_copy = remote(ms, mr, mx_send, mx_recv, dev(x_peer, j))
+    m_copy.start()
+    waits.append(m_copy)
+    for t in range(tiles):
+        at = pl.multiple_of(mine + t * tile, tile)
+        go[pl.ds(t * tile, tile), :] = dot(hid_t[pl.ds(at, tile), :], joined[...], 1, 0)
+    for k in range(chunks):
+        last_stage(k)
+    for t in range(tiles):
+        g_copies[t].wait_recv()
+        rows = pl.ds(t * tile, tile)
+        res = (go[rows, :] + gr[t].astype(f32)) * grad_scale
+        c_out[rows, :] = res[:, 0:BLOCK]
+        g_out[rows, :] = res[:, BLOCK:2 * BLOCK]
+    m_copy.wait_recv()
+    m_out[0] = (mixing + mr[...].astype(f32)) * grad_scale
+    for copy in w_copies + waits:
+        copy.wait_send()
+
+
+def fused(n_dp, hidden_in, content_weight, gating_weight, norm_gain, mixing_weight, mixing_bias, out_grad):
+    toks, depth = hidden_in.shape
+    shard, width = content_weight.shape
+    chunks = toks // BLOCK
+    nz = n_dp // 4
+    tile = 256
+    tiles = shard // tile
+    pieces = 2
+    grad_scale = 1.0 / math.sqrt(2 * toks)
+    bf16, f32 = jnp.bfloat16, jnp.float32
+    vmem = pl.BlockSpec(memory_space=pltpu.VMEM)
+    anywhere = pl.BlockSpec(memory_space=pl.ANY)
+    dma = pltpu.SemaphoreType.DMA
+    V = pltpu.VMEM
+    scratch = [
+        V((toks, depth), bf16), V((depth, toks), bf16), V((depth, 2 * width), bf16), V((toks, width), bf16),
+        V((toks, width), f32), V((toks, width), f32), V((toks, width), f32), V((toks, width), f32),
+        V((toks, width), f32), V((toks, width), bf16), V((toks, 2 * width), bf16),
+        V((8, toks // 2), f32), V((3, 8, toks // 2), f32), V((8, toks // 2), f32), V((nz - 1, 8, toks // 2), f32),
+        V((chunks, 2, 2, nz, BLOCK, width), bf16), V((chunks, 2, nz, BLOCK, width), bf16),
+        V((chunks, nz, BLOCK, width), bf16), V((chunks, nz, BLOCK, width), bf16),
+        V((chunks, nz - 1, BLOCK, width), bf16), V((chunks, nz - 1, BLOCK, width), bf16), V((chunks, BLOCK, width), f32),
+        V((tiles, tile, 2 * width), bf16), V((tiles, tile, 2 * width), bf16), V((shard, 2 * width), f32),
+        V((BLOCK, BLOCK), bf16), V((BLOCK, BLOCK), bf16),
+        dma((4,)), dma((2 * pieces,)), dma((2 * pieces,)), dma((3,)), dma((3,)), dma((nz - 1,)), dma((nz - 1,)),
+        dma((chunks,)), dma((chunks,)), dma((chunks,)), dma((chunks,)), dma((chunks, nz - 1)), dma((chunks, nz - 1)),
+        dma((tiles,)), dma((tiles,)), dma, dma,
+    ]
+    return pl.pallas_call(
+        functools.partial(fused_kernel, n_dp, width * n_dp, grad_scale),
+        out_shape=(
+            jax.ShapeDtypeStruct((toks, width), bf16),
+            jax.ShapeDtypeStruct((shard, width), f32),
+            jax.ShapeDtypeStruct((shard, width), f32),
+            jax.ShapeDtypeStruct(mixing_weight.shape, f32),
+        ),
+        in_specs=[anywhere, anywhere, anywhere, vmem, vmem, vmem, anywhere],
+        out_specs=(vmem,) * 4,
+        scratch_shapes=scratch,
+        compiler_params=pltpu.CompilerParams(
+            collective_id=0, has_side_effects=True, vmem_limit_bytes=40 * 1024 * 1024
+        ),
+    )(hidden_in, content_weight, gating_weight, norm_gain[None, :], mixing_weight, mixing_bias, out_grad)
+
+
+def fits(n_sp, n_dp, toks, shard, width):
+    paired = n_sp == 2 and n_dp % 4 == 0 and n_dp >= 8
+    return paired and width == GROUP_DIM and shard % 512 == 0 and toks % (2 * BLOCK) == 0 and toks <= shard
+
+
+def solve(*args):
+    n_sp, n_dp = lax.axis_size("sp"), lax.axis_size("dp")
+    shard, width = args[1].shape
+    if fits(n_sp, n_dp, args[0].shape[0], shard, width) and args[0].shape[1] == n_dp * width:
+        return fused(n_dp, *args)
+    return local(*args)
+
+
 def solution(mesh):
     in_specs = (
         P("sp", None),
@@ -119,4 +459,4 @@
         P("sp", "dp"),
     )
     out_specs = (P("sp", "dp"), P("sp", "dp"), P("sp", "dp"), P("dp", None, None))
-    return jax.shard_map(local, mesh=mesh, in_specs=in_specs, out_specs=out_specs, check_vma=False)
+    return jax.shard_map(solve, mesh=mesh, in_specs=in_specs, out_specs=out_specs, check_vma=False)

time: 172 us -> 56.8 us (0.33)
  waiting for transfers between devices: 63.8 us -> 0 us
  blocking collectives: 61.5 us -> 0 us
  Pallas kernels: 0 us -> 46.5 us
  between operations: 14.2 us -> 0.66 us
  matrix products: 9.04 us -> 0 us
  other arithmetic: 8.35 us -> 0 us
  local copies, waits for them, and re-layouts: 14.7 us -> 9.33 us
    unnamed x3 -> x0, waiting for transfers between devices: 62.4 us -> none
    pallas_call x0 -> x1, Pallas kernels: none -> 46.5 us  [fused(): pl.pallas_call(functools.partial(fused_kernel, n_dp, width * n_dp, grad_s...]
    psum x2 -> x0, blocking collectives: 41.4 us -> none  [the longest x1 33.1 us: local(): lax.psum((jnp.sum(gating, axis=1), jnp.sum(gating * gating, axis=1), jnp....]
    all_gather x2 -> x0, blocking collectives: 20.1 us -> none  [the longest x1 10.3 us: local(): lax.all_gather(content_weight, 'sp', axis=0, tiled=True)]
    dot_general x6 -> x0, matrix products: 9.04 us -> none  [the longest x1 2.66 us: hidden_term(): lax.dot_general(hidden_in, grads, (((0,), (0,)), ((), ())), preferred_ele...]
    reshape x3 -> x0, local copies, waits for them, and re-layouts: 3.87 us -> none  [the longest x1 1.77 us: local(): (mixed + jnp.transpose(mixing_bias)[None, :, :, None]).reshape(tok_rows,...]
    convert_element_type x3 -> x0, other arithmetic: 3.61 us -> none  [the longest x1 1.89 us: local(): normed = (centred * norm_gain[None, :]).astype(jnp.bfloat16)]
    reduce_sum x1 -> x0, other arithmetic: 2.25 us -> none  [local(): jnp.sum(gating, axis=1)]
  transfers between devices with their start and end apart: 2 -> 0, of which waited for: 2 -> 0; matrix products, arithmetic and copies ran while one was open for 6% -> 0% of each run, Pallas kernels for 0% -> 0%
where the time goes in v1:
time: 56.8 us; the launch traced here: 56.4 us
  Pallas kernels  46.5 us (82%)
  local copies, waits for them, and re-layouts  9.33 us (16%)
  between operations  0.66 us (1%)
    pallas_call x1, Pallas kernels, fused(): pl.pallas_call(functools.partial(fused_kernel, n_dp, width * n_dp, grad_s...  46.5 us
    unnamed x18, local copies, waits for them, and re-layouts  9.33 us

profile of v1, /device:TPU:0, one launch (start us, length us, event | category | flops | bytes accessed | tf_op | source)
XLA Modules:
  0.0 56.4 jit_solution(11416983859447874093)
XLA Ops:
  0.6 0.0 copy-start
  0.6 1.6 %copy-done = bf16[512,2048]{1,0:T(8,128)(2,1)S(1)} copy-done((bf16[512,2048]{1,0:T(8,128)(2,1)S(1)}, bf16[512,2048]{1,0:T(8,128)(2,1)}, u32[]{:S(2)}) %copy-start) | copy-done | bytes 2097176
  2.2 0.0 copy-start.1
  2.2 0.9 %copy-done.1 = bf16[1024,128]{1,0:T(8,128)(2,1)S(1)} copy-done((bf16[1024,128]{1,0:T(8,128)(2,1)S(1)}, bf16[1024,128]{1,0:T(8,128)(2,1)}, u32[]{:S(2)}) %copy-start.1) | copy-done | bytes 262168
  3.2 0.0 copy-start.2
  3.2 0.9 %copy-done.2 = bf16[1024,128]{1,0:T(8,128)(2,1)S(1)} copy-done((bf16[1024,128]{1,0:T(8,128)(2,1)S(1)}, bf16[1024,128]{1,0:T(8,128)(2,1)}, u32[]{:S(2)}) %copy-start.2) | copy-done | bytes 262168
  4.1 0.0 copy-start.3
  4.1 0.9 %copy-done.3 = bf16[512,128]{1,0:T(8,128)(2,1)S(1)} copy-done((bf16[512,128]{1,0:T(8,128)(2,1)S(1)}, bf16[512,128]{1,0:T(8,128)(2,1)}, u32[]{:S(2)}) %copy-start.3) | copy-done | bytes 131096
  5.0 0.0 copy-start.4
  5.0 0.8 %copy-done.4 = bf16[1,128,128]{2,1,0:T(8,128)(2,1)S(1)} copy-done((bf16[1,128,128]{2,1,0:T(8,128)(2,1)S(1)}, bf16[1,128,128]{2,1,0:T(8,128)(2,1)}, u32[]{:S(2)}) %copy-start.4) | copy-done | bytes 32792
  5.8 0.0 copy-start.5
  5.8 0.7 %copy-done.5 = f32[128]{0:T(128)S(1)} copy-done((f32[128]{0:T(128)S(1)}, f32[128]{0:T(128)}, u32[]{:S(2)}) %copy-start.5) | copy-done | bytes 536
  6.4 0.0 copy-start.6
  6.4 0.7 %copy-done.6 = f32[1,128]{1,0:T(1,128)S(1)} copy-done((f32[1,128]{1,0:T(1,128)S(1)}, f32[1,128]{1,0:T(1,128)}, u32[]{:S(2)}) %copy-start.6) | copy-done | bytes 536
  7.1 46.5 %shard_map.102 = (bf16[512,128]{1,0:T(8,128)(2,1)S(1)}, f32[1024,128]{1,0:T(8,128)S(1)}, f32[1024,128]{1,0:T(8,128)S(1)}, f32[1,128,128]{2,1,0:T(8,128)S(1)}) custom-call(bf16[512,2048]{1,0:T(8,128)(2,1)S(1)} %copy-done, bf16[1024,128]{1,0:T(8,128)(2,1)S(1)} %copy-done.1, bf16[1024,128]{1,0:T(8,128)(2,1)S(1)} %copy-done.2, f32[1,128]{1,0:T(1,128)S(1)} %bitcast.1, ...), custom_call_target="tpu_custom_call" | custom-call | tf_op jit(solution)/shard_map/pallas_call | solution.py:421
  53.6 0.7 %copy.15 = bf16[512,128]{1,0:T(8,128)(2,1)} copy(bf16[512,128]{1,0:T(8,128)(2,1)S(1)} %get-tuple-element.8) | data formatting | bytes 262144
  54.2 0.8 %copy.16 = f32[1024,128]{1,0:T(8,128)} copy(f32[1024,128]{1,0:T(8,128)S(1)} %get-tuple-element.9) | data formatting | bytes 1048576
  55.0 0.8 %copy.17 = f32[1024,128]{1,0:T(8,128)} copy(f32[1024,128]{1,0:T(8,128)S(1)} %get-tuple-element.10) | data formatting | bytes 1048576
  55.8 0.6 %copy.18 = f32[1,128,128]{2,1,0:T(8,128)} copy(f32[1,128,128]{2,1,0:T(8,128)S(1)} %get-tuple-element.11) | data formatting | bytes 131072
Async XLA Ops:
  0.6 1.6 %copy-start = (bf16[512,2048]{1,0:T(8,128)(2,1)S(1)}, bf16[512,2048]{1,0:T(8,128)(2,1)}, u32[]{:S(2)}) copy-start(bf16[512,2048]{1,0:T(8,128)(2,1)} %h_in.1) | copy-start | bytes 6291460
  2.2 0.9 %copy-start.1 = (bf16[1024,128]{1,0:T(8,128)(2,1)S(1)}, bf16[1024,128]{1,0:T(8,128)(2,1)}, u32[]{:S(2)}) copy-start(bf16[1024,128]{1,0:T(8,128)(2,1)} %wc_in.1) | copy-start | bytes 786436
  3.2 0.9 %copy-start.2 = (bf16[1024,128]{1,0:T(8,128)(2,1)S(1)}, bf16[1024,128]{1,0:T(8,128)(2,1)}, u32[]{:S(2)}) copy-start(bf16[1024,128]{1,0:T(8,128)(2,1)} %wg_in.1) | copy-start | bytes 786436
  4.1 0.9 %copy-start.3 = (bf16[512,128]{1,0:T(8,128)(2,1)S(1)}, bf16[512,128]{1,0:T(8,128)(2,1)}, u32[]{:S(2)}) copy-start(bf16[512,128]{1,0:T(8,128)(2,1)} %og_in.1) | copy-start | bytes 393220
  5.0 0.8 %copy-start.4 = (bf16[1,128,128]{2,1,0:T(8,128)(2,1)S(1)}, bf16[1,128,128]{2,1,0:T(8,128)(2,1)}, u32[]{:S(2)}) copy-start(bf16[1,128,128]{2,1,0:T(8,128)(2,1)} %mix_ref.1) | copy-start | bytes 98308
  5.8 0.7 %copy-start.5 = (f32[128]{0:T(128)S(1)}, f32[128]{0:T(128)}, u32[]{:S(2)}) copy-start(f32[128]{0:T(128)} %param.10) | copy-start | bytes 1540
  6.4 0.7 %copy-start.6 = (f32[1,128]{1,0:T(1,128)S(1)}, f32[1,128]{1,0:T(1,128)}, u32[]{:S(2)}) copy-start(f32[1,128]{1,0:T(1,128)} %bias_ref.1) | copy-start | bytes 1540

commit v2 on v1

--- a/solution.py
+++ b/solution.py
@@ -125,9 +125,9 @@
 
 def fused_kernel(
     n_dp, full_width, grad_scale,
-    h_in, wc_in, wg_in, gain_ref, mix_ref, bias_ref, og_in,
+    h_in, wc_in, wg_in, gain_in, mix_in, bias_in, og_in,
     x_out, c_out, g_out, m_out,
-    hid, hid_t, wts, og, cg, cg_t, cs, gat, slope_g, mg, joined,
+    gain_ref, mix_ref, bias_ref, hid, hid_t, wts, og, cg, cg_t, cs, gat, slope_g, mg, joined,
     stat_a, stat_quad, stat_b, stat_z,
     part, r_core, q_send, r_y, z_send, r_z, acc,
     gs, gr, go, ms, mr,
@@ -155,8 +155,11 @@
     j_y = j + 2 - 4 * y
     j_diag = j_core + 2 - 4 * y
 
+    mid = lax.rem((z + 1) // 2, 2)
+    z_xor = (z, z + 1 - 2 * lax.rem(z, 2), z + 2 - 4 * (z // 2), 3 - z)
+
     def z_dev(q):
-        return lax.rem(z + q, nz) * 4 + y * 2 + c
+        return z_xor[q] * 4 + y * 2 + c
 
     def dev(a, b):
         return {"sp": a, "dp": b}
@@ -174,6 +177,9 @@
         pltpu.make_async_copy(h_in, hid, load_sem.at[1]),
         pltpu.make_async_copy(wg_in, wts.at[pl.ds(mine, shard), pl.ds(BLOCK, BLOCK)], load_sem.at[2]),
         pltpu.make_async_copy(og_in, og, load_sem.at[3]),
+        pltpu.make_async_copy(gain_in, gain_ref, load_sem.at[4]),
+        pltpu.make_async_copy(mix_in, mix_ref, load_sem.at[5]),
+        pltpu.make_async_copy(bias_in, bias_ref, load_sem.at[6]),
     ]
     for load in loads:
         load.start()
@@ -202,12 +208,11 @@
     keep = lax.broadcasted_iota(jnp.int32, (BLOCK, BLOCK), 1) <= lax.broadcasted_iota(
         jnp.int32, (BLOCK, BLOCK), 0
     )
+    for load in loads:
+        load.wait()
     spatial = jnp.where(keep, mix_ref[0].astype(f32), 0.0).astype(bf16)
     gain = gain_ref[...]
     bias = jnp.broadcast_to(bias_ref[...], (BLOCK, BLOCK)).T
-
-    for load in loads:
-        load.wait()
     own = dot(hid[:, pl.ds(mine, shard)], wts[pl.ds(mine, shard), :], 1, 0)
     joined_pre = own
     acc_c = go.at[pl.ds(0, toks), pl.ds(0, BLOCK)]
@@ -299,19 +304,22 @@
     mixing = jnp.where(keep, mixing, 0.0)
 
     waits = []
-
-    def input_part(k):
-        grads = joined[pl.ds(k * BLOCK, BLOCK), :]
-        for zz in range(nz):
-            res = dot(grads, wts[pl.ds(zz * 4 * BLOCK, 4 * BLOCK), :], 1, 1).astype(bf16)
-            for yy in range(2):
-                for cc in range(2):
-                    at = (yy * 2 + cc) * BLOCK
-                    part[k, cc, yy, zz] = res[:, at:at + BLOCK]
-        copy = remote(part.at[k, 1 - c], r_core.at[k], core_send.at[k], core_recv.at[k], dev(i, j_core))
+    order = [(slot, h) for slot in range(nz) for h in range(2)]
+    pieces_in = len(order)
+
+    def input_part(n):
+        slot, h = order[n]
+        grads = joined[pl.ds(h * half, half), :]
+        at = pl.multiple_of(z_xor[3 - slot] * (4 * BLOCK), 4 * BLOCK)
+        res = dot(grads, wts[pl.ds(at, 4 * BLOCK), :], 1, 1).astype(bf16)
+        for yy in range(2):
+            for cc in range(2):
+                at = (yy * 2 + cc) * BLOCK
+                part[n, cc, yy] = res[:, at:at + BLOCK]
+        copy = remote(part.at[n, 1 - c], r_core.at[n], core_send.at[n], core_recv.at[n], dev(i, j_core))
         copy.start()
         waits.append(copy)
-        return copy
+        core_copies[n] = copy
 
     def weight_part(t):
         at = pl.multiple_of(theirs + t * tile, tile)
@@ -323,52 +331,78 @@
 
     core_copies, y_copies, z_copies, g_copies = {}, {}, {}, {}
 
-    def second_stage(k):
-        core_copies[k].wait_recv()
-        q_send[k] = (
-            part[k, c, 1 - y].astype(f32) + r_core[k, 1 - y].astype(f32)
-        ).astype(bf16)
-        copy = remote(q_send.at[k], r_y.at[k], y_send.at[k], y_recv.at[k], dev(i, j_y))
+    def second_stage(n):
+        core_copies[n].wait_recv()
+        q_send[n] = (part[n, c, 1 - y].astype(f32) + r_core[n, 1 - y].astype(f32)).astype(bf16)
+        copy = remote(q_send.at[n], r_y.at[n], y_send.at[n], y_recv.at[n], dev(i, j_y))
         copy.start()
         waits.append(copy)
-        y_copies[k] = copy
-
-    def third_stage(k):
-        y_copies[k].wait_recv()
-        z_copies[k] = []
-        for q in range(1, nz + 1):
-            zt = lax.rem(z + q, nz)
-            res = (
-                part[k, c, y, zt].astype(f32) + r_core[k, y, zt].astype(f32)
-            ) + r_y[k, zt].astype(f32)
-            if q == nz:
-                acc[k] = res
-                continue
-            z_send[k, q - 1] = res.astype(bf16)
-            copy = remote(
-                z_send.at[k, q - 1], r_z.at[k, q - 1], zz_send.at[k, q - 1], zz_recv.at[k, q - 1],
-                dev(i, z_dev(q)),
-            )
-            copy.start()
-            waits.append(copy)
-            z_copies[k].append(copy)
-
-    def last_stage(k):
-        res = acc[k]
-        for q in range(1, nz):
-            z_copies[k][q - 1].wait_recv()
-            res = res + r_z[k, q - 1].astype(f32)
-        x_out[pl.ds(k * BLOCK, BLOCK), :] = res.astype(bf16)
-
-    for step in range(max(chunks + 2, tiles)):
-        if step < chunks:
-            core_copies[step] = input_part(step)
+        y_copies[n] = copy
+
+    def direct(h):
+        return remote(z_send.at[0, h], r_z.at[0, h], zz_send.at[0, h], zz_recv.at[0, h], dev(i, z_dev(3)))
+
+    def relay(h):
+        return remote(z_send.at[0, h], r_z.at[3, h], zz_send.at[0, h], zz_recv.at[3, h], dev(i, z_dev(1)))
+
+    def third_stage(n):
+        slot, h = order[n]
+        y_copies[n].wait_recv()
+        res = (part[n, c, y].astype(f32) + r_core[n, y].astype(f32)) + r_y[n].astype(f32)
+        if slot == nz - 1:
+            acc[h] = res
+            return
+        if slot == 0:
+            z_send[0, h] = res.astype(bf16)
+
+            @pl.when(mid == 1)
+            def _():
+                direct(h).start()
+
+            @pl.when(mid == 0)
+            def _():
+                relay(h).start()
+
+            waits.append(direct(h))
+            return
+        if slot == 1:
+
+            @pl.when(mid == 1)
+            def _():
+                relay(h).wait_recv()
+                z_send[1, h] = (res + r_z[3, h].astype(f32)).astype(bf16)
+
+            @pl.when(mid == 0)
+            def _():
+                z_send[1, h] = res.astype(bf16)
+        else:
+            z_send[slot, h] = res.astype(bf16)
+        copy = remote(
+            z_send.at[slot, h], r_z.at[slot, h], zz_send.at[slot, h], zz_recv.at[slot, h], dev(i, z_dev(3 - slot))
+        )
+        copy.start()
+        waits.append(copy)
+        z_copies[slot, h] = copy
+
+    def last_stage(h):
+        @pl.when(mid == 1)
+        def _():
+            direct(h).wait_recv()
+            acc[h] = acc[h] + r_z[0, h].astype(f32)
+
+        res = acc[h]
+        for slot in range(1, nz - 1):
+            z_copies[slot, h].wait_recv()
+            res = res + r_z[slot, h].astype(f32)
+        x_out[pl.ds(h * half, half), :] = res.astype(bf16)
+
+    for step in range(pieces_in + 2):
+        if step < pieces_in:
+            input_part(step)
         if step < tiles:
             g_copies[step] = weight_part(step)
-        if 0 <= step - 1 < chunks:
-            second_stage(step - 1)
-        if 0 <= step - 2 < chunks:
-            third_stage(step - 2)
+        if step >= 2:
+            second_stage(step - 2)
     ms[...] = mixing.astype(bf16)
     m_copy = remote(ms, mr, mx_send, mx_recv, dev(x_peer, j))
     m_copy.start()
@@ -376,8 +410,10 @@
     for t in range(tiles):
         at = pl.multiple_of(mine + t * tile, tile)
         go[pl.ds(t * tile, tile), :] = dot(hid_t[pl.ds(at, tile), :], joined[...], 1, 0)
-    for k in range(chunks):
-        last_stage(k)
+    for n in range(pieces_in):
+        third_stage(n)
+    for h in range(2):
+        last_stage(h)
     for t in range(tiles):
         g_copies[t].wait_recv()
         rows = pl.ds(t * tile, tile)
@@ -393,7 +429,7 @@
 def fused(n_dp, hidden_in, content_weight, gating_weight, norm_gain, mixing_weight, mixing_bias, out_grad):
     toks, depth = hidden_in.shape
     shard, width = content_weight.shape
-    chunks = toks // BLOCK
+    half = toks // 2
     nz = n_dp // 4
     tile = 256
     tiles = shard // tile
@@ -405,17 +441,18 @@
     dma = pltpu.SemaphoreType.DMA
     V = pltpu.VMEM
     scratch = [
+        V((1, width), f32), V((1, BLOCK, BLOCK), bf16), V((1, BLOCK), f32),
         V((toks, depth), bf16), V((depth, toks), bf16), V((depth, 2 * width), bf16), V((toks, width), bf16),
         V((toks, width), f32), V((toks, width), f32), V((toks, width), f32), V((toks, width), f32),
         V((toks, width), f32), V((toks, width), bf16), V((toks, 2 * width), bf16),
         V((8, toks // 2), f32), V((3, 8, toks // 2), f32), V((8, toks // 2), f32), V((nz - 1, 8, toks // 2), f32),
-        V((chunks, 2, 2, nz, BLOCK, width), bf16), V((chunks, 2, nz, BLOCK, width), bf16),
-        V((chunks, nz, BLOCK, width), bf16), V((chunks, nz, BLOCK, width), bf16),
-        V((chunks, nz - 1, BLOCK, width), bf16), V((chunks, nz - 1, BLOCK, width), bf16), V((chunks, BLOCK, width), f32),
+        V((2 * nz, 2, 2, half, width), bf16), V((2 * nz, 2, half, width), bf16),
+        V((2 * nz, half, width), bf16), V((2 * nz, half, width), bf16),
+        V((nz - 1, 2, half, width), bf16), V((nz, 2, half, width), bf16), V((2, half, width), f32),
         V((tiles, tile, 2 * width), bf16), V((tiles, tile, 2 * width), bf16), V((shard, 2 * width), f32),
         V((BLOCK, BLOCK), bf16), V((BLOCK, BLOCK), bf16),
-        dma((4,)), dma((2 * pieces,)), dma((2 * pieces,)), dma((3,)), dma((3,)), dma((nz - 1,)), dma((nz - 1,)),
-        dma((chunks,)), dma((chunks,)), dma((chunks,)), dma((chunks,)), dma((chunks, nz - 1)), dma((chunks, nz - 1)),
+        dma((7,)), dma((2 * pieces,)), dma((2 * pieces,)), dma((3,)), dma((3,)), dma((nz - 1,)), dma((nz - 1,)),
+        dma((2 * nz,)), dma((2 * nz,)), dma((2 * nz,)), dma((2 * nz,)), dma((nz - 1, 2)), dma((nz, 2)),
         dma((tiles,)), dma((tiles,)), dma, dma,
     ]
     return pl.pallas_call(
@@ -426,17 +463,17 @@
             jax.ShapeDtypeStruct((shard, width), f32),
             jax.ShapeDtypeStruct(mixing_weight.shape, f32),
         ),
-        in_specs=[anywhere, anywhere, anywhere, vmem, vmem, vmem, anywhere],
+        in_specs=[anywhere] * 7,
         out_specs=(vmem,) * 4,
         scratch_shapes=scratch,
         compiler_params=pltpu.CompilerParams(
-            collective_id=0, has_side_effects=True, vmem_limit_bytes=40 * 1024 * 1024
+            collective_id=0, has_side_effects=True, vmem_limit_bytes=67043328
         ),
     )(hidden_in, content_weight, gating_weight, norm_gain[None, :], mixing_weight, mixing_bias, out_grad)
 
 
 def fits(n_sp, n_dp, toks, shard, width):
-    paired = n_sp == 2 and n_dp % 4 == 0 and n_dp >= 8
+    paired = n_sp == 2 and n_dp == 16
     return paired and width == GROUP_DIM and shard % 512 == 0 and toks % (2 * BLOCK) == 0 and toks <= shard
 
 

time: 56.8 us -> 51.6 us (0.908)
  local copies, waits for them, and re-layouts: 9.33 us -> 5.97 us
  Pallas kernels: 46.5 us -> 44.8 us
    unnamed x18 -> x6, local copies, waits for them, and re-layouts: 9.33 us -> 5.97 us
    pallas_call x1, Pallas kernels: 46.5 us -> 44.8 us  [fused(): pl.pallas_call(functools.partial(fused_kernel, n_dp, width * n_dp, grad_s...]
where the time goes in v2:
time: 51.6 us; the launch traced here: 51.4 us
  Pallas kernels  44.8 us (87%)
  local copies, waits for them, and re-layouts  5.97 us (12%)
  between operations  0.65 us (1%)
    pallas_call x1, Pallas kernels, fused(): pl.pallas_call(functools.partial(fused_kernel, n_dp, width * n_dp, grad_s...  44.8 us
    unnamed x6, local copies, waits for them, and re-layouts  5.97 us

profile of v2, /device:TPU:0, one launch (start us, length us, event | category | flops | bytes accessed | tf_op | source)
XLA Modules:
  0.0 51.4 jit_solution(10109922433247046077)
XLA Ops:
  0.6 44.8 %shard_map.102 = (bf16[512,128]{1,0:T(8,128)(2,1)}, f32[1024,128]{1,0:T(8,128)}, f32[1024,128]{1,0:T(8,128)}, f32[1,128,128]{2,1,0:T(8,128)}) custom-call(bf16[512,2048]{1,0:T(8,128)(2,1)} %h_in.1, bf16[1024,128]{1,0:T(8,128)(2,1)} %wc_in.1, bf16[1024,128]{1,0:T(8,128)(2,1)} %wg_in.1, f32[1,128]{1,0:T(1,128)} %bitcast.1, bf16[1,128,128]{2,1,0:T(8,128)(2,1)} %mix_in.1, ...), custom_call_target="tpu_custom_call" | custom-call | tf_op jit(solution)/shard_map/pallas_call | solution.py:458
  45.4 0.0 copy-start
  45.4 1.6 %copy.15 = bf16[512,128]{1,0:T(8,128)(2,1)} copy(bf16[512,128]{1,0:T(8,128)(2,1)} %get-tuple-element.8) | data formatting | bytes 262144
  47.0 1.9 %copy.16 = f32[1024,128]{1,0:T(8,128)} copy(f32[1024,128]{1,0:T(8,128)} %get-tuple-element.9) | data formatting | bytes 1048576
  48.9 1.9 %copy.17 = f32[1024,128]{1,0:T(8,128)} copy(f32[1024,128]{1,0:T(8,128)} %get-tuple-element.10) | data formatting | bytes 1048576
  50.8 0.0 copy-done
  50.8 0.6 %copy.18 = f32[1,128,128]{2,1,0:T(8,128)} copy(f32[1,128,128]{2,1,0:T(8,128)S(1)} %copy-done) | data formatting | bytes 131072
Async XLA Ops:
  45.4 5.3 %copy-start = (f32[1,128,128]{2,1,0:T(8,128)S(1)}, f32[1,128,128]{2,1,0:T(8,128)}, u32[]{:S(2)}) copy-start(f32[1,128,128]{2,1,0:T(8,128)} %get-tuple-element.11) | copy-start | bytes 196612

commit v3 on v2

--- a/solution.py
+++ b/solution.py
@@ -133,7 +133,7 @@
     gs, gr, go, ms, mr,
     load_sem, w_send, w_recv, sq_send, sq_recv, sz_send, sz_recv,
     core_send, core_recv, y_send, y_recv, zz_send, zz_recv,
-    gx_send, gx_recv, mx_send, mx_recv,
+    gx_send, gx_recv, mx_send, mx_recv, out_sem, x_buf, m_buf,
 ):
     toks = hid.shape[0]
     chunks = toks // BLOCK
@@ -304,6 +304,13 @@
     mixing = jnp.where(keep, mixing, 0.0)
 
     waits = []
+    stores = []
+
+    def store(src, dst):
+        copy = pltpu.make_async_copy(src, dst, out_sem.at[len(stores)])
+        copy.start()
+        stores.append(copy)
+
     order = [(slot, h) for slot in range(nz) for h in range(2)]
     pieces_in = len(order)
 
@@ -394,7 +401,8 @@
         for slot in range(1, nz - 1):
             z_copies[slot, h].wait_recv()
             res = res + r_z[slot, h].astype(f32)
-        x_out[pl.ds(h * half, half), :] = res.astype(bf16)
+        x_buf[pl.ds(h * half, half), :] = res.astype(bf16)
+        store(x_buf.at[pl.ds(h * half, half), :], x_out.at[pl.ds(h * half, half), :])
 
     for step in range(pieces_in + 2):
         if step < pieces_in:
@@ -412,18 +420,36 @@
         go[pl.ds(t * tile, tile), :] = dot(hid_t[pl.ds(at, tile), :], joined[...], 1, 0)
     for n in range(pieces_in):
         third_stage(n)
-    for h in range(2):
-        last_stage(h)
     for t in range(tiles):
         g_copies[t].wait_recv()
         rows = pl.ds(t * tile, tile)
-        res = (go[rows, :] + gr[t].astype(f32)) * grad_scale
-        c_out[rows, :] = res[:, 0:BLOCK]
-        g_out[rows, :] = res[:, BLOCK:2 * BLOCK]
+        go[rows, :] = (go[rows, :] + gr[t].astype(f32)) * grad_scale
+        store(go.at[rows, pl.ds(0, BLOCK)], c_out.at[rows, :])
+        store(go.at[rows, pl.ds(BLOCK, BLOCK)], g_out.at[rows, :])
     m_copy.wait_recv()
-    m_out[0] = (mixing + mr[...].astype(f32)) * grad_scale
+    m_buf[0] = (mixing + mr[...].astype(f32)) * grad_scale
+    store(m_buf, m_out)
+    for h in range(2):
+        last_stage(h)
+    for copy in stores:
+        copy.wait()
     for copy in w_copies + waits:
         copy.wait_send()
+
+
+def store_kernel(*refs):
+    count = len(refs) // 3
+    src, dst, held = refs[:count], refs[count:2 * count], refs[2 * count:3 * count]
+    sem = refs[-1]
+    loads = [pltpu.make_async_copy(src[k], held[k], sem.at[0, k]) for k in range(count)]
+    stores = [pltpu.make_async_copy(held[k], dst[k], sem.at[1, k]) for k in range(count)]
+    for load in loads:
+        load.start()
+    for load, store in zip(loads, stores):
+        load.wait()
+        store.start()
+    for store in stores:
+        store.wait()
 
 
 def fused(n_dp, hidden_in, content_weight, gating_weight, norm_gain, mixing_weight, mixing_bias, out_grad):
@@ -436,8 +462,7 @@
     pieces = 2
     grad_scale = 1.0 / math.sqrt(2 * toks)
     bf16, f32 = jnp.bfloat16, jnp.float32
-    vmem = pl.BlockSpec(memory_space=pltpu.VMEM)
-    anywhere = pl.BlockSpec(memory_space=pl.ANY)
+    in_hbm = pl.BlockSpec(memory_space=pltpu.HBM)
     dma = pltpu.SemaphoreType.DMA
     V = pltpu.VMEM
     scratch = [
@@ -453,9 +478,10 @@
         V((BLOCK, BLOCK), bf16), V((BLOCK, BLOCK), bf16),
         dma((7,)), dma((2 * pieces,)), dma((2 * pieces,)), dma((3,)), dma((3,)), dma((nz - 1,)), dma((nz - 1,)),
         dma((2 * nz,)), dma((2 * nz,)), dma((2 * nz,)), dma((2 * nz,)), dma((nz - 1, 2)), dma((nz, 2)),
-        dma((tiles,)), dma((tiles,)), dma, dma,
+        dma((tiles,)), dma((tiles,)), dma, dma, dma((2 * tiles + 3,)),
+        V((toks, width), bf16), V((1, BLOCK, BLOCK), f32),
     ]
-    return pl.pallas_call(
+    results = pl.pallas_call(
         functools.partial(fused_kernel, n_dp, width * n_dp, grad_scale),
         out_shape=(
             jax.ShapeDtypeStruct((toks, width), bf16),
@@ -463,13 +489,21 @@
             jax.ShapeDtypeStruct((shard, width), f32),
             jax.ShapeDtypeStruct(mixing_weight.shape, f32),
         ),
-        in_specs=[anywhere] * 7,
-        out_specs=(vmem,) * 4,
+        in_specs=[in_hbm] * 7,
+        out_specs=(in_hbm,) * 4,
         scratch_shapes=scratch,
         compiler_params=pltpu.CompilerParams(
             collective_id=0, has_side_effects=True, vmem_limit_bytes=67043328
         ),
     )(hidden_in, content_weight, gating_weight, norm_gain[None, :], mixing_weight, mixing_bias, out_grad)
+    return pl.pallas_call(
+        store_kernel,
+        out_shape=tuple(jax.ShapeDtypeStruct(r.shape, r.dtype) for r in results),
+        in_specs=[in_hbm] * 4,
+        out_specs=(in_hbm,) * 4,
+        scratch_shapes=[V(r.shape, r.dtype) for r in results] + [dma((2, 4))],
+        compiler_params=pltpu.CompilerParams(vmem_limit_bytes=67043328),
+    )(*results)
 
 
 def fits(n_sp, n_dp, toks, shard, width):

time: 51.6 us -> 47.3 us (0.917)
  local copies, waits for them, and re-layouts: 5.97 us -> 0 us
  Pallas kernels: 44.8 us -> 46.5 us
    unnamed x6 -> x0, local copies, waits for them, and re-layouts: 5.97 us -> none
    pallas_call x0 -> x1, Pallas kernels: none -> 2.16 us  [fused(): pl.pallas_call(store_kernel, out_shape=tuple((jax.ShapeDtypeStruct(r.shap...]
where the time goes in v3:
time: 47.3 us; the launch traced here: 47.1 us
  Pallas kernels  46.5 us (98%)
  between operations  0.64 us (1%)
    pallas_call x1, Pallas kernels, fused(): pl.pallas_call(functools.partial(fused_kernel, n_dp, width * n_dp, grad_s...  44.3 us
    pallas_call x1, Pallas kernels, fused(): pl.pallas_call(store_kernel, out_shape=tuple((jax.ShapeDtypeStruct(r.shap...  2.16 us

profile of v3, /device:TPU:0, one launch (start us, length us, event | category | flops | bytes accessed | tf_op | source)
XLA Modules:
  0.0 47.1 jit_solution(3372002332692115637)
XLA Ops:
  0.6 44.3 %shard_map.102 = (bf16[512,128]{1,0:T(8,128)(2,1)}, f32[1024,128]{1,0:T(8,128)}, f32[1024,128]{1,0:T(8,128)}, f32[1,128,128]{2,1,0:T(8,128)}) custom-call(bf16[512,2048]{1,0:T(8,128)(2,1)} %h_in.1, bf16[1024,128]{1,0:T(8,128)(2,1)} %wc_in.1, bf16[1024,128]{1,0:T(8,128)(2,1)} %wg_in.1, f32[1,128]{1,0:T(1,128)} %bitcast.1, bf16[1,128,128]{2,1,0:T(8,128)(2,1)} %mix_in.1, ...), custom_call_target="tpu_custom_call" | custom-call | tf_op jit(solution)/shard_map/pallas_call | solution.py:484
  45.0 2.2 %shard_map.103 = (bf16[512,128]{1,0:T(8,128)(2,1)}, f32[1024,128]{1,0:T(8,128)}, f32[1024,128]{1,0:T(8,128)}, f32[1,128,128]{2,1,0:T(8,128)}) custom-call(bf16[512,128]{1,0:T(8,128)(2,1)} %get-tuple-element.8.refs_0_, f32[1024,128]{1,0:T(8,128)} %get-tuple-element.9.refs_1_, f32[1024,128]{1,0:T(8,128)} %get-tuple-element.10.refs_2_, ...), custom_call_target="tpu_custom_call" | custom-call | tf_op jit(solution)/shard_map/pallas_call | solution.py:499
